TPU v7x, 32 devices: a whole 2x2x4 slice. The times are simulated.
32 devices in a mesh: ep: 8 (over z, core), tp: 4 (over y, x).
Axes of the slice: x: 2, y: 2, z: 4, core: 2. Of those that a mesh axis runs over, the one named last changes fastest.
Arguments:
- tokens: bfloat16 [1024, 2048], P('ep'), may hold values from -6 to 6
- chosen: int32 [8, 8, 8], replicated, may hold values from 0 to 127, as said below
- chosen_weight: float32 [8, 8, 8], P('ep'), may hold values from 0.1 to 1
- gate_weight: bfloat16 [8, 2048, 4096], P('ep', None, 'tp'), may hold values from -0.125 to 0.125
- up_weight: bfloat16 [8, 2048, 4096], P('ep', None, 'tp'), may hold values from -0.125 to 0.125
- down_weight: bfloat16 [8, 4096, 2048], P('ep', 'tp'), may hold values from -0.09375 to 0.09375
Outputs:
- combined: bfloat16 [1024, 2048], P('ep', 'tp')
Inputs may be any that keep to these rules, and one draw needn't show every extreme that they name: `chosen`: for every block and expert the 8 positions are distinct.
All inputs are finite; a program needn't handle non-finite values.
Results may differ from a plain program's by a relative error of at most 0.015.
Values may be sent and summed in bfloat16 or wider, within the bound.
A program may use at most 64 MiB of HBM per device.

v0:
```python
import jax
import jax.numpy as jnp
from jax import lax
from jax.sharding import PartitionSpec as P


def local(tokens, chosen, chosen_weight, gate_weight, up_weight, down_weight):
    ep_index = lax.axis_index("ep")
    tp_count = lax.axis_size("tp")
    tp_index = lax.axis_index("tp")
    tok_count, model_width = tokens.shape
    blocks, experts, picks_each = chosen.shape
    slice_width = model_width // tp_count
    columns = lax.dynamic_slice_in_dim(tokens, tp_index * slice_width, slice_width, 1)
    outgoing = lax.dynamic_index_in_dim(chosen, ep_index, 0, keepdims=False)
    leaving = jnp.take(columns, outgoing.reshape(-1), axis=0).reshape(
        experts, picks_each, slice_width
    )
    arrived = lax.all_to_all(leaving, "ep", split_axis=0, concat_axis=0, tiled=True).reshape(
        blocks * picks_each, slice_width
    )
    gate_local = gate_weight[0]
    up_local = up_weight[0]
    portion = lax.all_gather(arrived, "tp", axis=1, tiled=True)
    gate_sum = jnp.dot(portion, gate_local, preferred_element_type=jnp.float32)
    up_sum = jnp.dot(portion, up_local, preferred_element_type=jnp.float32)
    hidden = (jax.nn.silu(gate_sum) * up_sum).astype(jnp.bfloat16)
    down_local = down_weight[0].reshape(down_weight.shape[1], tp_count, slice_width)
    summed = lax.psum_scatter(
        jnp.einsum("rf,fcd->crd", hidden, down_local, preferred_element_type=jnp.float32).astype(
            jnp.bfloat16
        ),
        "tp",
        scatter_dimension=0,
        tiled=True,
    ).astype(jnp.float32)
    expert_out = summed[0].astype(jnp.bfloat16).reshape(blocks, picks_each, slice_width)
    returned = lax.all_to_all(expert_out, "ep", split_axis=0, concat_axis=0, tiled=True).reshape(
        experts * picks_each, slice_width
    )
    positions = jnp.arange(tok_count, dtype=jnp.int32)[:, None]
    placement_matrix = jnp.where(
        outgoing.reshape(1, -1) == positions, chosen_weight[0].reshape(1, -1), 0.0
    )
    combined = jnp.dot(
        placement_matrix,
        returned.astype(jnp.float32),
        precision=lax.Precision.HIGHEST,
        preferred_element_type=jnp.float32,
    )
    return combined.astype(jnp.bfloat16)


def solution(mesh):
    return jax.shard_map(
        local,
        mesh=mesh,
        in_specs=(
            P("ep", None),
            P(),
            P("ep", None, None),
            P("ep", None, "tp"),
            P("ep", None, "tp"),
            P("ep", "tp", None),
        ),
        out_specs=P("ep", "tp"),
        check_vma=False,
    )
```

profile of v0, /device:TPU:0, one launch (start us, length us, event | category | flops | bytes accessed | tf_op | source)
XLA Modules:
  0.0 84.8 jit_solution(2384732761228838541)
XLA Ops:
  6.5 0.0 copy-start
  6.5 0.8 compare_and_fusion
  7.3 0.1 reshape.58
  7.4 0.2 copy-done
  7.6 0.7 gather_fusion
  8.3 0.7 bitcast_select_fusion
  9.0 6.4 %all-to-all-start = ((bf16[8,8,512]{2,1,0:T(8,128)(2,1)}), bf16[8,8,512]{2,1,0:T(8,128)(2,1)S(1)}, u32[]{:S(2)}, u32[]{:S(2)}) async-start(bf16[8,8,512]{2,1,0:T(8,128)(2,1)} %bitcast_select_fusion), calls=%async_computation | async-start | bytes 131072 | tf_op jit(solution)/shard_map/all_to_all | solution.py:19
  15.4 0.0 reduce-scatter.4.cloned.1.call-start
  15.4 7.8 %reshape_squeeze.4 = bf16[1024,4,512]{2,1,0:T(4,128)(2,1)} reshape(bf16[1,1024,2048]{2,1,0:T(8,128)(2,1)} %param.11) | data formatting | bytes 8388608 | tf_op jit(solution)/shard_map/reshape;squeeze | solution.py:28
  23.2 0.0 all-to-all-done
  23.2 9.0 %all_gather.3 = bf16[64,2048]{1,0:T(8,128)(2,1)S(1)} all-gather(bf16[64,512]{1,0:T(8,128)(2,1)S(1)} %bitcast.36), channel_id=1, replica_groups=mesh['ep'=8,'tp'=4] {'tp'}, dimensions={1}, use_global_device_ids=true | all-gather | bytes 327680 | tf_op jit(solution)/shard_map/all_gather | solution.py:24
  32.2 3.0 %fusion.2 = f32[64,1024]{1,0:T(8,128)S(1)} fusion(bf16[64,2048]{1,0:T(8,128)(2,1)S(1)} %all_gather.3, bf16[1,2048,1024]{2,1,0:T(8,128)(2,1)} %param.9), kind=kOutput, calls=%fused_computation.3 | convolution fusion | flops 268435456 | bytes 4718592 | tf_op jit(solution)/shard_map/dot_general | solution.py:25
  35.2 0.0 copy-start.1
  35.2 6.3 %fusion.12 = bf16[4,64,512]{2,1,0:T(8,128)(2,1)} fusion(bf16[1024,4,512]{2,1,0:T(4,128)(2,1)} %reshape_squeeze.4, bf16[64,2048]{1,0:T(8,128)(2,1)S(1)} %all_gather.3, bf16[1,2048,1024]{2,1,0:T(8,128)(2,1)} %param.10, f32[64,1024]{1,0:T(8,128)S(1)} %fusion.2), kind=kOutput, calls=%fused_computation.9 | convolution fusion | flops 537395200 | bytes 9175040 | tf_op jit(solution)/shard_map/rf,fcd->crd/dot_general | solution.py:30
  41.6 0.0 reduce-scatter.4.cloned.1.call-update
  41.6 25.0 %reduce-scatter.4.cloned.1.call-done = bf16[1,64,512]{2,1,0:T(8,128)(2,1)} async-done(((bf16[4,64,512]{2,1,0:T(8,128)(2,1)}), bf16[1,64,512]{2,1,0:T(8,128)(2,1)}) %reduce-scatter.4.cloned.1.call-update) | async-done | bytes 65552
  66.6 4.6 %all-to-all-start.1 = ((bf16[8,8,512]{2,1,0:T(8,128)(2,1)}), bf16[8,8,512]{2,1,0:T(8,128)(2,1)S(1)}, u32[]{:S(2)}, u32[]{:S(2)}) async-start(bf16[8,8,512]{2,1,0:T(8,128)(2,1)} %bitcast.37), calls=%async_computation.1 | async-start | bytes 131072 | tf_op jit(solution)/shard_map/all_to_all | solution.py:38
  71.2 0.1 eq.17
  71.3 0.0 copy-done.1
  71.3 0.1 broadcast_in_dim.25
  71.3 5.8 %all-to-all-done.1 = bf16[8,8,512]{2,1,0:T(8,128)(2,1)S(1)} async-done(((bf16[8,8,512]{2,1,0:T(8,128)(2,1)}), bf16[8,8,512]{2,1,0:T(8,128)(2,1)S(1)}, u32[]{:S(2)}, u32[]{:S(2)}) %all-to-all-start.1) | async-done | bytes 65568 | tf_op jit(solution)/shard_map/all_to_all | solution.py:38
  77.1 0.9 %convolution_convert_fusion = bf16[128,512]{1,0:T(8,128)(2,1)} fusion(bf16[8,8,512]{2,1,0:T(8,128)(2,1)S(1)} %all-to-all-done.1, f32[64]{0:T(128)S(1)} %broadcast_in_dim.25, s32[64]{0:T(128)S(1)} %eq.17), kind=kOutput, calls=%fused_computation.11 | convolution fusion | flops 50413568 | bytes 197120 | tf_op jit(solution)/shard_map/dot_general | solution.py:45
  (3 shorter events, 0.0 us)
Async XLA Ops:
  6.5 1.1 %copy-start = (bf16[128,2048]{1,0:T(8,128)(2,1)S(1)}, bf16[128,2048]{1,0:T(8,128)(2,1)}, u32[]{:S(2)}) copy-start(bf16[128,2048]{1,0:T(8,128)(2,1)} %param.6) | copy-start | bytes 1572868
  9.0 14.2 %all-to-all-start = ((bf16[8,8,512]{2,1,0:T(8,128)(2,1)}), bf16[8,8,512]{2,1,0:T(8,128)(2,1)S(1)}, u32[]{:S(2)}, u32[]{:S(2)}) async-start(bf16[8,8,512]{2,1,0:T(8,128)(2,1)} %bitcast_select_fusion), calls=%async_computation | async-start | bytes 131072 | tf_op jit(solution)/shard_map/all_to_all | solution.py:19
  15.4 51.2 %reduce-scatter.4.cloned.1.call-start = ((), (), s32[]{:S(2)}) async-start(), calls=%async_computation.3 | async-start | bytes 327680
  35.2 36.0 %copy-start.1 = (f32[1,8,8]{2,1,0:T(8,128)S(1)}, f32[1,8,8]{2,1,0:T(8,128)}, u32[]{:S(2)}) copy-start(f32[1,8,8]{2,1,0:T(8,128)} %param.8) | copy-start | bytes 772
  66.6 10.5 %all-to-all-start.1 = ((bf16[8,8,512]{2,1,0:T(8,128)(2,1)}), bf16[8,8,512]{2,1,0:T(8,128)(2,1)S(1)}, u32[]{:S(2)}, u32[]{:S(2)}) async-start(bf16[8,8,512]{2,1,0:T(8,128)(2,1)} %bitcast.37), calls=%async_computation.1 | async-start | bytes 131072 | tf_op jit(solution)/shard_map/all_to_all | solution.py:38
Sparse Core Ops, SparseCore 0:
  41.7 24.7 reduce-scatter.3
where the time goes:
time: 85.3 us; the launch traced here: 84.8 us
  waiting for transfers between devices  30.7 us (36%)
  between operations  13.4 us (16%)
  starting transfers between devices  11 us (13%)
  matrix products  10.3 us (12%)
  blocking collectives  8.98 us (11%)
  local copies, waits for them, and re-layouts  8.96 us (11%)
  other arithmetic  1.48 us (2%)
    unnamed x2, waiting for transfers between devices  25 us
    all_gather x1, blocking collectives, local(): portion = lax.all_gather(arrived, 'tp', axis=1, tiled=True)  8.98 us
    another operation x1, local copies, waits for them, and re-layouts, local(): down_weight[0].reshape(down_weight.shape[1], tp_count, slice_width)  7.8 us
    all_to_all x1, starting transfers between devices, local(): lax.all_to_all(leaving, 'ep', split_axis=0, concat_axis=0, tiled=True)  6.35 us
    dot_general x1, matrix products, local(): jnp.einsum('rf,fcd->crd', hidden, down_local, preferred_element_type=jnp....  6.33 us
    all_to_all x1, waiting for transfers between devices, local(): lax.all_to_all(expert_out, 'ep', split_axis=0, concat_axis=0, tiled=True)  5.76 us
    all_to_all x1, starting transfers between devices, local(): lax.all_to_all(expert_out, 'ep', split_axis=0, concat_axis=0, tiled=True)  4.61 us
    dot_general x1, matrix products, local(): gate_sum = jnp.dot(portion, gate_local, preferred_element_type=jnp.float32)  3.03 us
  transfers between devices with their start and end apart: 3, of which 2 were waited for; matrix products, arithmetic and copies ran while one was open for 9% of the time, Pallas kernels for 0%

commit v1 on v0

--- a/solution.py
+++ b/solution.py
@@ -2,6 +2,29 @@
 import jax.numpy as jnp
 from jax import lax
 from jax.sharding import PartitionSpec as P
+
+
+def cut_along(x, dim, count):
+    shape = x.shape
+    blocks = x.reshape(*shape[:dim], count, shape[dim] // count, *shape[dim + 1 :])
+    return jnp.moveaxis(blocks, dim, 0)
+
+
+def laid_out(tiles, dim):
+    shape = list(tiles.shape[1:])
+    shape[dim] *= tiles.shape[0]
+    return jnp.moveaxis(tiles, 0, dim).reshape(shape)
+
+
+def sent_to_each(x, axis, split_dim, concat_dim):
+    size, index = (lax.axis_size(axis), lax.axis_index(axis))
+    blocks = cut_along(x, split_dim, size)
+    outs = [blocks[index]]
+    for step in range(1, size):
+        sent = blocks[(index + step) % size]
+        outs.append(lax.ppermute(sent, axis, [(i, (i + step) % size) for i in range(size)]))
+    blocks = jnp.stack(outs)[(index - jnp.arange(size)) % size]
+    return laid_out(blocks, concat_dim)
 
 
 def local(tokens, chosen, chosen_weight, gate_weight, up_weight, down_weight):
@@ -16,9 +39,7 @@
     leaving = jnp.take(columns, outgoing.reshape(-1), axis=0).reshape(
         experts, picks_each, slice_width
     )
-    arrived = lax.all_to_all(leaving, "ep", split_axis=0, concat_axis=0, tiled=True).reshape(
-        blocks * picks_each, slice_width
-    )
+    arrived = sent_to_each(leaving, "ep", 0, 0).reshape(blocks * picks_each, slice_width)
     gate_local = gate_weight[0]
     up_local = up_weight[0]
     portion = lax.all_gather(arrived, "tp", axis=1, tiled=True)

time: 85.3 us -> 93.1 us (1.091)
  waiting for transfers between devices: 30.7 us -> 36.9 us
  starting transfers between devices: 11 us -> 12.5 us
    ppermute x0 -> x7, waiting for transfers between devices: none -> 9.42 us  [sent_to_each(): lax.ppermute(sent, axis, [(i, (i + step) % size) for i in range(size)])]
    ppermute x0 -> x7, starting transfers between devices: none -> 7.9 us  [sent_to_each(): lax.ppermute(sent, axis, [(i, (i + step) % size) for i in range(size)])]
    all_to_all x1 -> x0, starting transfers between devices: 6.35 us -> none  [local(): lax.all_to_all(leaving, 'ep', split_axis=0, concat_axis=0, tiled=True)]
    unnamed x2, waiting for transfers between devices: 25 us -> 21.8 us
  transfers between devices with their start and end apart: 3 -> 9, of which waited for: 2 -> 4; matrix products, arithmetic and copies ran while one was open for 9% -> 9% of each run, Pallas kernels for 0% -> 0%
where the time goes in v1:
time: 93.1 us; the launch traced here: 92.6 us
  waiting for transfers between devices  36.9 us (40%)
  between operations  13.5 us (15%)
  starting transfers between devices  12.5 us (13%)
  matrix products  10.3 us (11%)
  local copies, waits for them, and re-layouts  9.52 us (10%)
  blocking collectives  8.99 us (10%)
    unnamed x2, waiting for transfers between devices  21.8 us
    ppermute x7, waiting for transfers between devices, sent_to_each(): lax.ppermute(sent, axis, [(i, (i + step) % size) for i in range(size)])  9.42 us
    all_gather x1, blocking collectives, local(): portion = lax.all_gather(arrived, 'tp', axis=1, tiled=True)  8.99 us
    ppermute x7, starting transfers between devices, sent_to_each(): lax.ppermute(sent, axis, [(i, (i + step) % size) for i in range(size)])  7.9 us
    another operation x1, local copies, waits for them, and re-layouts, local(): down_weight[0].reshape(down_weight.shape[1], tp_count, slice_width)  7.81 us
    dot_general x1, matrix products, local(): jnp.einsum('rf,fcd->crd', hidden, down_local, preferred_element_type=jnp....  6.33 us
    all_to_all x1, waiting for transfers between devices, local(): lax.all_to_all(expert_out, 'ep', split_axis=0, concat_axis=0, tiled=True)  5.76 us
    all_to_all x1, starting transfers between devices, local(): lax.all_to_all(expert_out, 'ep', split_axis=0, concat_axis=0, tiled=True)  4.62 us
  transfers between devices with their start and end apart: 9, of which 4 were waited for; matrix products, arithmetic and copies ran while one was open for 9% of the time, Pallas kernels for 0%

profile of v1, /device:TPU:0, one launch (start us, length us, event | category | flops | bytes accessed | tf_op | source)
XLA Modules:
  0.0 92.6 jit_solution(522080417674637723)
XLA Ops:
  6.5 0.8 compare_and_fusion
  7.3 0.1 reshape.114
  7.4 0.2 copy-done
  7.6 0.7 gather_fusion
  8.3 0.1 bitcast_select_fusion
  8.4 4.6 %collective-permute-start.6 = (bf16[1,8,512]{2,1,0:T(8,128)(2,1)S(1)}, bf16[1,8,512]{2,1,0:T(8,128)(2,1)S(1)}, u32[]{:S(2)}, u32[]{:S(2)}) collective-permute-start(bf16[1,8,512]{2,1,0:T(8,128)(2,1)S(1)} %get-tuple-element.7), channel_id=1, source_target_pairs={{0,28},{4,0},{8,4},{12,8},{16,12},{20,16},{24,20},{28,24},{1,29},{... | collective-permute-start | bytes 24584 | tf_op jit(solution)/shard_map/ppermute | solution.py:25
  13.0 0.6 collective-permute-start.5
  13.6 0.0 collective-permute-start.4
  13.6 2.7 %collective-permute-start.3 = (bf16[1,8,512]{2,1,0:T(8,128)(2,1)S(1)}, bf16[1,8,512]{2,1,0:T(8,128)(2,1)S(1)}, u32[]{:S(2)}, u32[]{:S(2)}) collective-permute-start(bf16[1,8,512]{2,1,0:T(8,128)(2,1)S(1)} %get-tuple-element.10), channel_id=1, source_target_pairs={{0,16},{4,20},{8,24},{12,28},{16,0},{20,4},{24,8},{28,12},{1,17},{... | collective-permute-start | bytes 24584 | tf_op jit(solution)/shard_map/ppermute | solution.py:25
  16.3 0.0 collective-permute-start
  16.3 7.8 %reshape_squeeze.4 = bf16[1024,4,512]{2,1,0:T(4,128)(2,1)} reshape(bf16[1,1024,2048]{2,1,0:T(8,128)(2,1)} %param.11) | data formatting | bytes 8388608 | tf_op jit(solution)/shard_map/reshape;squeeze | solution.py:49
  24.2 0.0 collective-permute-done
  24.2 0.0 collective-permute-start.1
  24.2 5.4 %collective-permute-done.1 = bf16[1,8,512]{2,1,0:T(8,128)(2,1)S(1)} collective-permute-done((bf16[1,8,512]{2,1,0:T(8,128)(2,1)S(1)}, bf16[1,8,512]{2,1,0:T(8,128)(2,1)S(1)}, u32[]{:S(2)}, u32[]{:S(2)}) %collective-permute-start.1) | collective-permute-done | bytes 8224 | tf_op jit(solution)/shard_map/ppermute | solution.py:25
  29.6 0.0 collective-permute-start.2
  29.6 4.0 %collective-permute-done.2 = bf16[1,8,512]{2,1,0:T(8,128)(2,1)S(1)} collective-permute-done((bf16[1,8,512]{2,1,0:T(8,128)(2,1)S(1)}, bf16[1,8,512]{2,1,0:T(8,128)(2,1)S(1)}, u32[]{:S(2)}, u32[]{:S(2)}) %collective-permute-start.2) | collective-permute-done | bytes 8224 | tf_op jit(solution)/shard_map/ppermute | solution.py:25
  33.6 0.0 collective-permute-done.3
  33.6 0.0 collective-permute-done.4
  33.6 0.0 collective-permute-done.5
  33.6 0.0 collective-permute-done.6
  33.7 0.6 gather_fusion.1
  34.2 9.0 %all_gather.3 = bf16[64,2048]{1,0:T(8,128)(2,1)S(1)} all-gather(bf16[64,512]{1,0:T(8,128)(2,1)S(1)} %bitcast.67), channel_id=1, replica_groups=mesh['ep'=8,'tp'=4] {'tp'}, dimensions={1}, use_global_device_ids=true | all-gather | bytes 327680 | tf_op jit(solution)/shard_map/all_gather | solution.py:45
  43.2 3.0 %fusion.2 = f32[64,1024]{1,0:T(8,128)S(1)} fusion(bf16[64,2048]{1,0:T(8,128)(2,1)S(1)} %all_gather.3, bf16[1,2048,1024]{2,1,0:T(8,128)(2,1)} %param.9), kind=kOutput, calls=%fused_computation.4 | convolution fusion | flops 268435456 | bytes 4718592 | tf_op jit(solution)/shard_map/dot_general | solution.py:46
  46.2 0.0 copy-start.1
  46.2 6.3 %fusion.12 = bf16[4,64,512]{2,1,0:T(8,128)(2,1)} fusion(bf16[1024,4,512]{2,1,0:T(4,128)(2,1)} %reshape_squeeze.4, bf16[64,2048]{1,0:T(8,128)(2,1)S(1)} %all_gather.3, bf16[1,2048,1024]{2,1,0:T(8,128)(2,1)} %param.10, f32[64,1024]{1,0:T(8,128)S(1)} %fusion.2), kind=kOutput, calls=%fused_computation.10 | convolution fusion | flops 537395200 | bytes 9175040 | tf_op jit(solution)/shard_map/rf,fcd->crd/dot_general | solution.py:51
  52.6 0.0 reduce-scatter.4.cloned.1.call-update
  52.6 21.7 %reduce-scatter.4.cloned.1.call-done = bf16[1,64,512]{2,1,0:T(8,128)(2,1)} async-done(((bf16[4,64,512]{2,1,0:T(8,128)(2,1)}), bf16[1,64,512]{2,1,0:T(8,128)(2,1)}) %reduce-scatter.4.cloned.1.call-update) | async-done | bytes 65552
  74.3 4.6 %all-to-all-start = ((bf16[8,8,512]{2,1,0:T(8,128)(2,1)}), bf16[8,8,512]{2,1,0:T(8,128)(2,1)S(1)}, u32[]{:S(2)}, u32[]{:S(2)}) async-start(bf16[8,8,512]{2,1,0:T(8,128)(2,1)} %bitcast.69), calls=%async_computation | async-start | bytes 131072 | tf_op jit(solution)/shard_map/all_to_all | solution.py:59
  79.0 0.1 eq.27
  79.0 0.1 broadcast_in_dim.26
  79.1 5.8 %all-to-all-done = bf16[8,8,512]{2,1,0:T(8,128)(2,1)S(1)} async-done(((bf16[8,8,512]{2,1,0:T(8,128)(2,1)}), bf16[8,8,512]{2,1,0:T(8,128)(2,1)S(1)}, u32[]{:S(2)}, u32[]{:S(2)}) %all-to-all-start) | async-done | bytes 65568 | tf_op jit(solution)/shard_map/all_to_all | solution.py:59
  84.9 0.9 convolution_convert_fusion
  (16 shorter events, 0.1 us)
Async XLA Ops:
  6.5 1.1 %copy-start = (bf16[128,2048]{1,0:T(8,128)(2,1)S(1)}, bf16[128,2048]{1,0:T(8,128)(2,1)}, u32[]{:S(2)}) copy-start(bf16[128,2048]{1,0:T(8,128)(2,1)} %param.6) | copy-start | bytes 1572868
  6.5 67.8 %reduce-scatter.4.cloned.1.call-start = ((), (), s32[]{:S(2)}) async-start(), calls=%async_computation.2 | async-start | bytes 327680
  8.4 25.2 %collective-permute-start.6 = (bf16[1,8,512]{2,1,0:T(8,128)(2,1)S(1)}, bf16[1,8,512]{2,1,0:T(8,128)(2,1)S(1)}, u32[]{:S(2)}, u32[]{:S(2)}) collective-permute-start(bf16[1,8,512]{2,1,0:T(8,128)(2,1)S(1)} %get-tuple-element.7), channel_id=1, source_target_pairs={{0,28},{4,0},{8,4},{12,8},{16,12},{20,16},{24,20},{28,24},{1,29},{... | collective-permute-start | bytes 24584 | tf_op jit(solution)/shard_map/ppermute | solution.py:25
  13.0 20.6 %collective-permute-start.5 = (bf16[1,8,512]{2,1,0:T(8,128)(2,1)S(1)}, bf16[1,8,512]{2,1,0:T(8,128)(2,1)S(1)}, u32[]{:S(2)}, u32[]{:S(2)}) collective-permute-start(bf16[1,8,512]{2,1,0:T(8,128)(2,1)S(1)} %get-tuple-element.8), channel_id=1, source_target_pairs={{0,24},{4,28},{8,0},{12,4},{16,8},{20,12},{24,16},{28,20},{1,25},{... | collective-permute-start | bytes 24584 | tf_op jit(solution)/shard_map/ppermute | solution.py:25
  13.6 20.0 %collective-permute-start.4 = (bf16[1,8,512]{2,1,0:T(8,128)(2,1)S(1)}, bf16[1,8,512]{2,1,0:T(8,128)(2,1)S(1)}, u32[]{:S(2)}, u32[]{:S(2)}) collective-permute-start(bf16[1,8,512]{2,1,0:T(8,128)(2,1)S(1)} %get-tuple-element.9), channel_id=1, source_target_pairs={{0,20},{4,24},{8,28},{12,0},{16,4},{20,8},{24,12},{28,16},{1,21},{... | collective-permute-start | bytes 24584 | tf_op jit(solution)/shard_map/ppermute | solution.py:25
  13.6 20.0 %collective-permute-start.3 = (bf16[1,8,512]{2,1,0:T(8,128)(2,1)S(1)}, bf16[1,8,512]{2,1,0:T(8,128)(2,1)S(1)}, u32[]{:S(2)}, u32[]{:S(2)}) collective-permute-start(bf16[1,8,512]{2,1,0:T(8,128)(2,1)S(1)} %get-tuple-element.10), channel_id=1, source_target_pairs={{0,16},{4,20},{8,24},{12,28},{16,0},{20,4},{24,8},{28,12},{1,17},{... | collective-permute-start | bytes 24584 | tf_op jit(solution)/shard_map/ppermute | solution.py:25
  16.3 7.8 %collective-permute-start = (bf16[1,8,512]{2,1,0:T(8,128)(2,1)S(1)}, bf16[1,8,512]{2,1,0:T(8,128)(2,1)S(1)}, u32[]{:S(2)}, u32[]{:S(2)}) collective-permute-start(bf16[1,8,512]{2,1,0:T(8,128)(2,1)S(1)} %get-tuple-element.13), channel_id=1, source_target_pairs={{0,4},{4,8},{8,12},{12,16},{16,20},{20,24},{24,28},{28,0},{1,5},{5... | collective-permute-start | bytes 24584 | tf_op jit(solution)/shard_map/ppermute | solution.py:25
  24.2 5.4 %collective-permute-start.1 = (bf16[1,8,512]{2,1,0:T(8,128)(2,1)S(1)}, bf16[1,8,512]{2,1,0:T(8,128)(2,1)S(1)}, u32[]{:S(2)}, u32[]{:S(2)}) collective-permute-start(bf16[1,8,512]{2,1,0:T(8,128)(2,1)S(1)} %get-tuple-element.12), channel_id=1, source_target_pairs={{0,8},{4,12},{8,16},{12,20},{16,24},{20,28},{24,0},{28,4},{1,9},{5... | collective-permute-start | bytes 24584 | tf_op jit(solution)/shard_map/ppermute | solution.py:25
  29.6 4.0 %collective-permute-start.2 = (bf16[1,8,512]{2,1,0:T(8,128)(2,1)S(1)}, bf16[1,8,512]{2,1,0:T(8,128)(2,1)S(1)}, u32[]{:S(2)}, u32[]{:S(2)}) collective-permute-start(bf16[1,8,512]{2,1,0:T(8,128)(2,1)S(1)} %get-tuple-element.11), channel_id=1, source_target_pairs={{0,12},{4,16},{8,20},{12,24},{16,28},{20,0},{24,4},{28,8},{1,13},{... | collective-permute-start | bytes 24584 | tf_op jit(solution)/shard_map/ppermute | solution.py:25
  46.2 32.8 %copy-start.1 = (f32[1,8,8]{2,1,0:T(8,128)S(1)}, f32[1,8,8]{2,1,0:T(8,128)}, u32[]{:S(2)}) copy-start(f32[1,8,8]{2,1,0:T(8,128)} %param.8) | copy-start | bytes 772
  74.3 10.5 %all-to-all-start = ((bf16[8,8,512]{2,1,0:T(8,128)(2,1)}), bf16[8,8,512]{2,1,0:T(8,128)(2,1)S(1)}, u32[]{:S(2)}, u32[]{:S(2)}) async-start(bf16[8,8,512]{2,1,0:T(8,128)(2,1)} %bitcast.69), calls=%async_computation | async-start | bytes 131072 | tf_op jit(solution)/shard_map/all_to_all | solution.py:59
Sparse Core Ops, SparseCore 0:
  52.7 21.5 reduce-scatter.3
